TPU v7x, 512 devices: a whole 4x4x16 slice. The times are simulated.
512 devices in a mesh: ep: 32 (over z, core), tp: 16 (over y, x).
Axes of the slice: x: 4, y: 4, z: 16, core: 2. Of those that a mesh axis runs over, the one named last changes fastest.
Arguments:
- attn_rows: bfloat16 [4096, 2048], P('ep'), may hold values from -6 to 6
- attn_gain: float32 [2048], replicated, may hold values from 0.1 to 1.9
- query_weight: bfloat16 [2048, 1024], P(None, 'tp'), may hold values from -0.125 to 0.125
- key_weight: bfloat16 [2048, 1024], P(None, 'tp'), may hold values from -0.125 to 0.125
- value_weight: bfloat16 [2048, 1024], P(None, 'tp'), may hold values from -0.125 to 0.125
- key_bias: bfloat16 [16, 4096], P('tp', 'ep'), may hold values from -14 to 0
- out_weight: bfloat16 [1024, 2048], P(None, 'tp'), may hold values from -0.75 to 0.75
- expert_rows: bfloat16 [4096, 2048], P('ep'), may hold values from -6 to 6
- expert_gain: float32 [2048], replicated, may hold values from 0.1 to 1.9
- expert_ids: int32 [4096, 2], P('ep'), may hold values from 0 to 31, all different within a row; in each aligned block of 128 rows (0 to 127, 128 to 255, ...) at most 16 rows name the same one
- group_logits: float32 [4096, 4], P('ep'), may hold values from -6 to 6
- pair_logits: float32 [4096, 2], P('ep'), may hold values from -6 to 6
- gate_weight: bfloat16 [32, 2048, 2048], P('ep', None, 'tp'), may hold values from -0.125 to 0.125
- up_weight: bfloat16 [32, 2048, 2048], P('ep', None, 'tp'), may hold values from -0.125 to 0.125
- down_weight: bfloat16 [32, 2048, 2048], P('ep', None, 'tp'), may hold values from -0.125 to 0.125
Outputs:
- mixed: bfloat16 [4096, 2048], P('ep', 'tp')
- expert_out: bfloat16 [4096, 2048], P('ep', 'tp')
Inputs may be any that keep to these rules, and one draw needn't show every extreme that they name: `expert_ids`: each row names two different experts; in every aligned block of 128 rows no expert is named more than 16 times.
All inputs are finite; a program needn't handle non-finite values.
Results may differ from a plain program's by a relative error of at most 0.0083.
Values may be sent and summed in bfloat16 or wider, within the bound.
No kernel may reach another device: no remote copies, remote signals or barrier semaphores. Data moves between devices by JAX's collectives and lax.ppermute only.
A program may use at most 64 MiB of HBM per device.

v0:
```python
import jax
import jax.numpy as jnp
from jax import lax
from jax.sharding import PartitionSpec as P

EXPERTS = 32
GROUPS = 4
GROUP_SIZE = 8
CAP = 16
epsilon = 1e-06


def sent_together(arrays, axis, dim, along):
    widths = [a.shape[along] for a in arrays]
    both = jnp.concatenate(arrays, axis=along)
    filled = lax.all_gather(both, axis, axis=dim, tiled=True)
    return tuple(jnp.split(filled, [sum(widths[:k]) for k in range(1, len(widths))], axis=along))


def laid_out(tiles, dim):
    lengths = list(tiles.shape[1:])
    lengths[dim] *= tiles.shape[0]
    return jnp.moveaxis(tiles, 0, dim).reshape(lengths)


def sent_to_all(shard, axis):
    copies = jnp.broadcast_to(shard, (lax.axis_size(axis), *shard.shape))
    return lax.all_to_all(copies, axis, split_axis=0, concat_axis=0, tiled=True)


def collect(shard, axis, dim):
    return laid_out(sent_to_all(shard, axis), dim)


def norm_rows(rows, gain):
    values = rows.astype(jnp.float32)
    scaled = values * lax.rsqrt(jnp.mean(values * values, axis=-1, keepdims=True) + epsilon)
    return (scaled * gain).astype(jnp.bfloat16)


def shards(
    attn_rows,
    attn_gain,
    query_weight,
    key_weight,
    value_weight,
    key_bias,
    out_weight,
    expert_rows,
    expert_gain,
    expert_ids,
    group_logits,
    pair_logits,
    gate_weight,
    up_weight,
    down_weight,
):
    rows_dev = attn_rows.shape[0]
    blocks = lax.axis_size("ep")
    own_start = lax.axis_index("ep") * rows_dev
    heads_local = key_bias.shape[0]
    head_size = query_weight.shape[1] // heads_local
    width_local = heads_local * head_size
    scale = head_size ** (-0.5)
    normed = norm_rows(attn_rows, attn_gain)
    query = jnp.dot(normed, query_weight, preferred_element_type=jnp.float32).astype(jnp.bfloat16)
    query = query.reshape(rows_dev, heads_local, head_size)
    keys = jnp.dot(normed, key_weight, preferred_element_type=jnp.float32).astype(jnp.bfloat16)
    values = jnp.dot(normed, value_weight, preferred_element_type=jnp.float32).astype(jnp.bfloat16)
    pairs = jnp.concatenate([keys, values], axis=1)
    bias_rows = key_bias.T
    query_pos = own_start + jnp.arange(rows_dev)
    init = (
        jnp.zeros((blocks, heads_local, rows_dev), jnp.float32),
        jnp.zeros((blocks, heads_local, rows_dev, head_size), jnp.float32),
    )
    piece = sent_together((pairs, bias_rows), "ep", 0, 1)

    def work(state):
        pair_rows, bias_piece = piece
        count = pair_rows.shape[0]
        spans = count // rows_dev
        key_part = pair_rows[:, :width_local].reshape(count, heads_local, head_size)
        value_part = pair_rows[:, width_local:].reshape(spans, rows_dev, heads_local, head_size)
        scores = (
            jnp.einsum("thd,shd->hts", query, key_part, preferred_element_type=jnp.float32) * scale
        )
        scores = scores + bias_piece.T.astype(jnp.float32)[:, None, :]
        scores = scores.reshape(heads_local, rows_dev, spans, rows_dev)
        causal = jnp.arange(count)[None, :] < query_pos[:, None]
        causal = causal.reshape(rows_dev, spans, rows_dev)
        negative_part = jax.nn.log_sigmoid(-scores)
        log_keep = jnp.where(causal, negative_part, 0.0)
        suffix = lax.cumsum(log_keep, axis=3, reverse=True) - log_keep
        weights = jnp.where(causal, jnp.exp(scores + negative_part + suffix), 0.0).astype(
            jnp.bfloat16
        )
        block_out = jnp.einsum(
            "htnr,nrhd->nhtd", weights, value_part, preferred_element_type=jnp.float32
        )
        block_keep = jnp.transpose(jnp.sum(log_keep, axis=3), (2, 0, 1))
        return (block_keep, block_out)

    def untouched(state):
        return state

    totals, outputs = lax.cond(jnp.int32(0) < own_start + rows_dev, work, untouched, init)
    later = lax.cumsum(totals, axis=0, reverse=True) - totals
    merged = jnp.sum(jnp.exp(later)[..., None] * outputs, axis=0)
    attended = jnp.transpose(merged, (1, 0, 2)).reshape(rows_dev, width_local).astype(jnp.bfloat16)
    mixed = jnp.dot(
        lax.all_gather(attended, "tp", axis=1, tiled=True),
        out_weight,
        preferred_element_type=jnp.float32,
    )
    mixed = mixed.astype(jnp.bfloat16)
    normed = norm_rows(expert_rows, expert_gain)
    width = normed.shape[1]
    cols_local = down_weight.shape[2]
    flattened = expert_ids.reshape(-1)
    picks = flattened.shape[0]
    marks = (flattened[:, None] == jnp.arange(EXPERTS)[None, :]).astype(jnp.int32)
    position = jnp.sum((jnp.cumsum(marks, axis=0) - marks) * marks, axis=1)
    source = jnp.arange(picks) // 2
    send = (
        jnp.zeros((EXPERTS, CAP, width), jnp.bfloat16).at[flattened, position].set(normed[source])
    )
    send = send.reshape(blocks, EXPERTS // blocks, CAP, width)
    shares = jnp.exp(group_logits)
    shares = shares / jnp.sum(shares, axis=1, keepdims=True)
    groups = expert_ids // GROUP_SIZE
    group_marks = (groups[:, :, None] == jnp.arange(GROUPS)[None, None, :]).astype(jnp.float32)
    chosen = jnp.sum(shares[:, None, :] * group_marks, axis=2)
    spread = pair_logits[:, 0] - pair_logits[:, 1]
    pair_share = jnp.stack([jax.nn.sigmoid(spread), jax.nn.sigmoid(-spread)], axis=1)
    route_weights = chosen * pair_share
    narrow = lax.dynamic_slice_in_dim(send, lax.axis_index("tp") * cols_local, cols_local, 3)
    add_piece = collect(
        lax.all_to_all(narrow, "ep", split_axis=0, concat_axis=0, tiled=True), "tp", 3
    )
    gate = jnp.einsum("secd,edf->secf", add_piece, gate_weight, preferred_element_type=jnp.float32)
    up = jnp.einsum("secd,edf->secf", add_piece, up_weight, preferred_element_type=jnp.float32)
    hidden = (jax.nn.silu(gate) * up).astype(jnp.bfloat16)
    result = jnp.einsum(
        "secf,efd->secd", collect(hidden, "tp", 3), down_weight, preferred_element_type=jnp.float32
    ).astype(jnp.bfloat16)
    back = lax.all_to_all(result, "ep", split_axis=0, concat_axis=0, tiled=True).reshape(
        EXPERTS, CAP, cols_local
    )
    picked = back[flattened, position].reshape(expert_rows.shape[0], 2, cols_local)
    combined = jnp.sum(route_weights[:, :, None] * picked.astype(jnp.float32), axis=1)
    expert_out = combined.astype(jnp.bfloat16)
    return (mixed, expert_out)


def solution(mesh):
    placed = (
        P("ep", None),
        P(),
        P(None, "tp"),
        P(None, "tp"),
        P(None, "tp"),
        P("tp", "ep"),
        P(None, "tp"),
        P("ep", None),
        P(),
        P("ep", None),
        P("ep", None),
        P("ep", None),
        P("ep", None, "tp"),
        P("ep", None, "tp"),
        P("ep", None, "tp"),
    )
    return jax.shard_map(
        shards,
        mesh=mesh,
        in_specs=placed,
        out_specs=(P("ep", "tp"), P("ep", "tp")),
        check_vma=False,
    )
```

profile of v0, /device:TPU:2, one launch (start us, length us, event | category | flops | bytes accessed | tf_op | source)
XLA Modules:
  0.0 225.2 jit_solution(5643384250437827587)
XLA Ops:
  7.2 0.8 copy.86
  8.5 1.2 fusion.28
  10.7 1.2 fusion.30
  11.9 2.3 %gather_fusion = bf16[256,2048]{1,0:T(8,128)(2,1)} fusion(bf16[128,2048]{1,0:T(8,128)(2,1)S(1)} %fusion.30, s32[1024]{0:T(1024)S(1)} %pad_clamp_fusion), kind=kCustom, calls=%fused_computation | custom fusion | bytes 2098176 | tf_op jit(solution)/shard_map/gather | solution.py:126
  14.5 33.3 %scatter_fusion = bf16[32,16,2048]{2,1,0:T(8,128)(2,1)S(1)} fusion(bf16[32,16,2048]{2,1,0:T(8,128)(2,1)S(1)} %broadcast_in_dim.21, s32[256]{0:T(256)S(1)} %bitcast.129, bf16[256,2048]{1,0:T(8,128)(2,1)} %gather_fusion), kind=kCustom, calls=%fused_computation.2 | custom fusion | bytes 3147776 | tf_op jit(solution)/shard_map/scatter | solution.py:126
  47.9 32.5 %all_to_all.23 = bf16[32,1,16,128]{3,2,1,0:T(8,128)(2,1)S(1)} all-to-all(bf16[32,1,16,128]{3,2,1,0:T(8,128)(2,1)S(1)} %dynamic-slice_bitcast_fusion), channel_id=1, replica_groups=mesh['ep'=32,'tp'=16] {'ep'}, dimensions={0} | all-to-all | bytes 262144 | tf_op jit(solution)/shard_map/all_to_all | solution.py:139
  80.3 1.8 broadcast_in_dim.22
  82.1 7.6 %all-to-all-start.1 = ((bf16[16,32,1,16,128]{4,3,1,2,0:T(8,128)(2,1)}), bf16[16,32,1,16,128]{4,3,1,2,0:T(8,128)(2,1)S(1)}, u32[]{:S(2)}, u32[]{:S(2)}) async-start(bf16[16,32,1,16,128]{4,3,1,2,0:T(8,128)(2,1)} %broadcast_in_dim.22), calls=%async_computation.1 | async-start | bytes 4194304 | tf_op jit(solution)/shard_map/all_to_all | solution.py:28
  90.4 1.3 convolution_convert_fusion.4
  92.3 23.6 %all-to-all-done.1 = bf16[16,32,1,16,128]{4,3,1,2,0:T(8,128)(2,1)S(1)} async-done(((bf16[16,32,1,16,128]{4,3,1,2,0:T(8,128)(2,1)}), bf16[16,32,1,16,128]{4,3,1,2,0:T(8,128)(2,1)S(1)}, u32[]{:S(2)}, u32[]{:S(2)}) %all-to-all-start.1) | async-done | bytes 2097184 | tf_op jit(solution)/shard_map/all_to_all | solution.py:28
  115.9 3.8 %copy.90 = bf16[32,1,16,16,128]{4,3,2,0,1:T(8,128)(2,1)} copy(bf16[32,1,16,16,128]{4,2,0,1,3:T(8,128)(2,1)S(1)} %bitcast.131) | data formatting | bytes 4194304 | tf_op jit(solution)/shard_map/transpose | solution.py:23
  119.7 2.8 %reshape.363 = bf16[32,16,2048]{2,1,0:T(8,128)(2,1)S(1)} reshape(bf16[32,1,16,16,128]{4,3,2,0,1:T(8,128)(2,1)} %copy.90) | data formatting | bytes 4194304 | tf_op jit(solution)/shard_map/reshape.28
  122.6 0.7 convolution_bitcast_fusion.2
  124.3 1.7 broadcast_in_dim.23
  126.0 8.0 %all-to-all-start.2 = ((bf16[16,32,1,16,128]{4,3,1,2,0:T(8,128)(2,1)}), bf16[16,32,1,16,128]{4,3,1,2,0:T(8,128)(2,1)}, u32[]{:S(2)}, u32[]{:S(2)}) async-start(bf16[16,32,1,16,128]{4,3,1,2,0:T(8,128)(2,1)} %broadcast_in_dim.23), calls=%async_computation.2 | async-start | bytes 4194304 | tf_op jit(solution)/shard_map/all_to_all | solution.py:28
  134.7 19.1 %all-gather.2.cloned.1.call-done = bf16[4096,129]{0,1:T(8,128)(2,1)} async-done(((bf16[128,129]{0,1:T(8,128)(2,1)}), bf16[4096,129]{0,1:T(8,128)(2,1)}) %all-gather.2.cloned.1.call-update) | async-done | bytes 1056784 | tf_op jit(solution)/shard_map/all_gather | solution.py:16
  153.8 19.2 %conditional.1 = (f32[32,1,128,64]{2,3,0,1:T(8,128)}, f32[32,1,128]{2,1,0:T(1,128)S(1)}) conditional(s32[]{:T(128)} %convert_element_type.82, () %tuple.16, (s32[]{:T(128)}, s32[128]{0:T(128)S(1)}, bf16[4096,129]{0,1:T(8,128)(2,1)}, bf16[128,64]{0,1:T(8,128)(2,1)S(1)}) %tuple.17), branch_computations={%region_1.0_spmd, %region_2.5_spmd} | conditional | flops 219160704 | bytes 19064852 | solution.py:107
  153.8 0.8 slice_convert_fusion
  154.7 1.5 fusion.11
  156.6 1.4 fusion.4
  158.1 2.4 %copy.79 = f32[128,32,128]{0,1,2:T(8,128)} copy(f32[128,32,128]{2,1,0:T(8,128)S(1)} %bitcast.128) | data formatting | bytes 4194304 | tf_op jit(solution)/shard_map/cond/branch_1_fun/reshape | solution.py:89
  160.5 9.9 %fusion.1 = bf16[128,32,128]{0,1,2:T(8,128)(2,1)S(1)} fusion(f32[128,32,128]{0,1,2:T(8,128)} %copy.79, s32[128]{0:T(128)S(1)} %broadcast_add_fusion, s32[32,128]{0,1:T(8,128)S(1)} %multiply_add_fusion), kind=kOutput, calls=%fused_computation.9 | output fusion | flops 78643200 | bytes 3162624 | tf_op jit(solution)/shard_map/cond/branch_1_fun/reduce_window_sum | solution.py:94
  170.4 2.6 %convolution_bitcast_fusion = f32[32,1,128,64]{2,3,0,1:T(8,128)} fusion(bf16[128,32,128]{0,1,2:T(8,128)(2,1)S(1)} %fusion.1, bf16[4096,129]{0,1:T(8,128)(2,1)} %get-tuple-element.17), kind=kOutput, calls=%fused_computation.22 | convolution fusion | flops 67108864 | bytes 2621440 | tf_op jit(solution)/shard_map/cond/branch_1_fun/htnr,nrhd->nhtd/dot_general | solution.py:98
  173.0 4.0 %copy.91 = bf16[32,1,16,16,128]{4,3,2,0,1:T(8,128)(2,1)S(1)} copy(bf16[32,1,16,16,128]{4,2,0,1,3:T(8,128)(2,1)} %bitcast.26) | data formatting | bytes 4194304 | tf_op jit(solution)/shard_map/transpose | solution.py:23
  177.0 2.3 %reshape.366 = bf16[32,16,2048]{2,1,0:T(8,128)(2,1)} reshape(bf16[32,1,16,16,128]{4,3,2,0,1:T(8,128)(2,1)S(1)} %copy.91) | data formatting | bytes 4194304 | tf_op jit(solution)/shard_map/reshape.35
  179.4 3.0 %fusion.22 = bf16[32,1,16,128]{3,2,1,0:T(8,128)(2,1)} fusion(bf16[32,16,2048]{2,1,0:T(8,128)(2,1)} %reshape.366, bf16[1,2048,128]{2,1,0:T(8,128)(2,1)S(1)} %copy-done.2), kind=kOutput, calls=%fused_computation.44 | convolution fusion | flops 268500992 | bytes 2752512 | tf_op jit(solution)/shard_map/secf,efd->secd/dot_general | solution.py:144
  182.4 7.3 %all-to-all-start.3 = ((bf16[32,1,16,128]{3,2,1,0:T(8,128)(2,1)}), bf16[32,1,16,128]{3,2,1,0:T(8,128)(2,1)S(1)}, u32[]{:S(2)}, u32[]{:S(2)}) async-start(bf16[32,1,16,128]{3,2,1,0:T(8,128)(2,1)} %fusion.22), calls=%async_computation.3 | async-start | bytes 262144 | tf_op jit(solution)/shard_map/all_to_all | solution.py:147
  189.8 1.3 multiply_reduce_fusion
  191.1 23.8 %all_gather.7 = bf16[128,1024]{0,1:T(8,128)(2,1)S(1)} all-gather(bf16[128,64]{0,1:T(8,128)(2,1)S(1)} %multiply_reduce_fusion), channel_id=1, replica_groups=mesh['ep'=32,'tp'=16] {'tp'}, dimensions={1}, use_global_device_ids=true | all-gather | bytes 278528 | tf_op jit(solution)/shard_map/all_gather | solution.py:112
  214.9 0.9 convolution_convert_fusion.1
  215.8 1.7 gather_fusion.1
  217.5 0.9 fusion.34
  (63 shorter events, 5.1 us)
Async XLA Ops:
  7.2 115.4 %copy-start = (bf16[1,2048,128]{2,1,0:T(8,128)(2,1)S(1)}, bf16[1,2048,128]{2,1,0:T(8,128)(2,1)}, u32[]{:S(2)}) copy-start(bf16[1,2048,128]{2,1,0:T(8,128)(2,1)} %param.29) | copy-start | bytes 1572868
  82.1 7.7 %copy-start.1 = (bf16[128,2048]{1,0:T(8,128)(2,1)S(1)}, bf16[128,2048]{1,0:T(8,128)(2,1)}, u32[]{:S(2)}) copy-start(bf16[128,2048]{1,0:T(8,128)(2,1)} %param.17) | copy-start | bytes 1572868
  82.1 7.9 %copy-start.9 = (bf16[2048,64]{0,1:T(8,128)(2,1)S(1)}, bf16[2048,64]{0,1:T(8,128)(2,1)}, u32[]{:S(2)}) copy-start(bf16[2048,64]{0,1:T(8,128)(2,1)} %param.21) | copy-start | bytes 786436
  82.1 7.9 %copy-start.11 = (f32[2048]{0:T(1024)S(1)}, f32[2048]{0:T(1024)}, u32[]{:S(2)}) copy-start(f32[2048]{0:T(1024)} %param.18) | copy-start | bytes 24580
  82.1 33.8 %all-to-all-start.1 = ((bf16[16,32,1,16,128]{4,3,1,2,0:T(8,128)(2,1)}), bf16[16,32,1,16,128]{4,3,1,2,0:T(8,128)(2,1)S(1)}, u32[]{:S(2)}, u32[]{:S(2)}) async-start(bf16[16,32,1,16,128]{4,3,1,2,0:T(8,128)(2,1)} %broadcast_in_dim.22), calls=%async_computation.1 | async-start | bytes 4194304 | tf_op jit(solution)/shard_map/all_to_all | solution.py:28
  89.7 2.0 copy-start.7
  89.7 64.1 %all-gather.2.cloned.1.call-start = ((), (), s32[]{:S(2)}) async-start(), calls=%async_computation.4 | async-start | bytes 1148928 | tf_op jit(solution)/shard_map/all_gather | solution.py:16
  122.5 1.0 copy-start.8
  126.0 8.0 %copy-start.4 = (f32[128,4]{0,1:T(4,128)S(1)}, f32[128,4]{0,1:T(4,128)}, u32[]{:S(2)}) copy-start(f32[128,4]{0,1:T(4,128)} %param.27) | copy-start | bytes 6148
  126.0 8.1 %copy-start.5 = (s32[128,2]{0,1:T(2,128)S(1)}, s32[128,2]{0,1:T(2,128)}, u32[]{:S(2)}) copy-start(s32[128,2]{0,1:T(2,128)} %param.26) | copy-start | bytes 3076
  126.0 8.1 %copy-start.6 = (f32[128,2]{0,1:T(2,128)S(1)}, f32[128,2]{0,1:T(2,128)}, u32[]{:S(2)}) copy-start(f32[128,2]{0,1:T(2,128)} %param.28) | copy-start | bytes 3076
  126.0 8.3 %copy-start.10 = (bf16[2048,64]{0,1:T(8,128)(2,1)S(1)}, bf16[2048,64]{0,1:T(8,128)(2,1)}, u32[]{:S(2)}) copy-start(bf16[2048,64]{0,1:T(8,128)(2,1)} %param.19) | copy-start | bytes 786436
  126.0 47.0 %all-to-all-start.2 = ((bf16[16,32,1,16,128]{4,3,1,2,0:T(8,128)(2,1)}), bf16[16,32,1,16,128]{4,3,1,2,0:T(8,128)(2,1)}, u32[]{:S(2)}, u32[]{:S(2)}) async-start(bf16[16,32,1,16,128]{4,3,1,2,0:T(8,128)(2,1)} %broadcast_in_dim.23), calls=%async_computation.2 | async-start | bytes 4194304 | tf_op jit(solution)/shard_map/all_to_all | solution.py:28
  177.0 2.3 %copy-start.2 = (bf16[1,2048,128]{2,1,0:T(8,128)(2,1)S(1)}, bf16[1,2048,128]{2,1,0:T(8,128)(2,1)}, u32[]{:S(2)}) copy-start(bf16[1,2048,128]{2,1,0:T(8,128)(2,1)} %param.31) | copy-start | bytes 1572868
  179.4 35.5 %copy-start.3 = (bf16[1024,128]{1,0:T(8,128)(2,1)S(1)}, bf16[1024,128]{1,0:T(8,128)(2,1)}, u32[]{:S(2)}) copy-start(bf16[1024,128]{1,0:T(8,128)(2,1)} %param.23) | copy-start | bytes 786436
  182.4 33.4 %all-to-all-start.3 = ((bf16[32,1,16,128]{3,2,1,0:T(8,128)(2,1)}), bf16[32,1,16,128]{3,2,1,0:T(8,128)(2,1)S(1)}, u32[]{:S(2)}, u32[]{:S(2)}) async-start(bf16[32,1,16,128]{3,2,1,0:T(8,128)(2,1)} %fusion.22), calls=%async_computation.3 | async-start | bytes 262144 | tf_op jit(solution)/shard_map/all_to_all | solution.py:147
Sparse Core Ops, SparseCore 0:
  92.6 61.1 all-gather.1
where the time goes:
time: 227 us; the launch traced here: 225 us
  local copies, waits for them, and re-layouts  58.8 us (26%)
  blocking collectives  56.3 us (25%)
  waiting for transfers between devices  42.7 us (19%)
  starting transfers between devices  23 us (10%)
  other arithmetic  18.6 us (8%)
  between operations  14.3 us (6%)
  matrix products  11.5 us (5%)
    scatter x1, local copies, waits for them, and re-layouts, shards(): jnp.zeros((EXPERTS, CAP, width), jnp.bfloat16).at[flattened, position]  33.3 us
    all_to_all x1, blocking collectives, shards(): lax.all_to_all(narrow, 'ep', split_axis=0, concat_axis=0, tiled=True)  32.5 us
    all_gather x1, blocking collectives, shards(): lax.all_gather(attended, 'tp', axis=1, tiled=True)  23.8 us
    all_to_all x2, waiting for transfers between devices, sent_to_all(): return lax.all_to_all(copies, axis, split_axis=0, concat_axis=0, tiled=True)  23.6 us
    all_gather x1, waiting for transfers between devices, sent_together(): filled = lax.all_gather(both, axis, axis=dim, tiled=True)  19.1 us
    all_to_all x2, starting transfers between devices, sent_to_all(): return lax.all_to_all(copies, axis, split_axis=0, concat_axis=0, tiled=True)  15.6 us
    another operation x1, other arithmetic, work(): suffix = lax.cumsum(log_keep, axis=3, reverse=True) - log_keep  9.92 us
    transpose x2, local copies, waits for them, and re-layouts, laid_out(): return jnp.moveaxis(tiles, 0, dim).reshape(lengths)  7.81 us
  transfers between devices with their start and end apart: 4, of which 2 were waited for; matrix products, arithmetic and copies ran while one was open for 15% of the time, Pallas kernels for 0%

commit v1 on v0

--- a/solution.py
+++ b/solution.py
@@ -8,6 +8,20 @@
 GROUP_SIZE = 8
 CAP = 16
 epsilon = 1e-06
+
+
+def sums_all_apply(u):
+    dev_n = lax.axis_size("tp")
+    by_place = tuple(((it, (it + 1) % dev_n) for it in range(dev_n)))
+    all_rows = tuple(((it, (it - 1) % dev_n) for it in range(dev_n)))
+    carry_in, row_out = ([u], [u])
+    for _ in range(dev_n // 2):
+        carry_in.append(lax.ppermute(carry_in[-1], "tp", by_place))
+    for _ in tuple(range((dev_n - 1) // 2)):
+        small = lax.ppermute(row_out[-1], "tp", all_rows)
+        row_out.append(small)
+    item_now = jnp.concatenate([*carry_in[::-1], *row_out[1:]], 1)
+    return jnp.roll(item_now, (lax.axis_index("tp") - dev_n // 2) * u.shape[1], 1)
 
 
 def sent_together(arrays, axis, dim, along):
@@ -108,11 +122,7 @@
     later = lax.cumsum(totals, axis=0, reverse=True) - totals
     merged = jnp.sum(jnp.exp(later)[..., None] * outputs, axis=0)
     attended = jnp.transpose(merged, (1, 0, 2)).reshape(rows_dev, width_local).astype(jnp.bfloat16)
-    mixed = jnp.dot(
-        lax.all_gather(attended, "tp", axis=1, tiled=True),
-        out_weight,
-        preferred_element_type=jnp.float32,
-    )
+    mixed = jnp.dot(sums_all_apply(attended), out_weight, preferred_element_type=jnp.float32)
     mixed = mixed.astype(jnp.bfloat16)
     normed = norm_rows(expert_rows, expert_gain)
     width = normed.shape[1]

time: 227 us -> 290 us (1.28)
  the two profiles are of different devices: /device:TPU:2 before, /device:TPU:1 now
where the time goes in v1:
time: 290 us; the launch traced here: 288 us
  starting transfers between devices  106 us (37%)
  waiting for transfers between devices  72.4 us (25%)
  local copies, waits for them, and re-layouts  64 us (22%)
  other arithmetic  17.7 us (6%)
  between operations  15 us (5%)
  matrix products  13.1 us (5%)
    ppermute x7, starting transfers between devices, sums_all_apply(): small = lax.ppermute(row_out[-1], 'tp', all_rows)  46.8 us
    scatter x1, local copies, waits for them, and re-layouts, shards(): jnp.zeros((EXPERTS, CAP, width), jnp.bfloat16).at[flattened, position]  33.3 us
    all_to_all x2, waiting for transfers between devices, sent_to_all(): return lax.all_to_all(copies, axis, split_axis=0, concat_axis=0, tiled=True)  22.3 us
    all_gather x1, waiting for transfers between devices, sent_together(): filled = lax.all_gather(both, axis, axis=dim, tiled=True)  21.1 us
    ppermute x8, starting transfers between devices, sums_all_apply(): carry_in.append(lax.ppermute(carry_in[-1], 'tp', by_place))  16.8 us
    all_to_all x1, starting transfers between devices, shards(): lax.all_to_all(narrow, 'ep', split_axis=0, concat_axis=0, tiled=True)  16.7 us
    all_to_all x1, starting transfers between devices, shards(): lax.all_to_all(result, 'ep', split_axis=0, concat_axis=0, tiled=True)  15.6 us
    ppermute x7, waiting for transfers between devices, sums_all_apply(): small = lax.ppermute(row_out[-1], 'tp', all_rows)  13.6 us
  transfers between devices with their start and end apart: 20, of which 5 were waited for; matrix products, arithmetic and copies ran while one was open for 27% of the time, Pallas kernels for 0%

profile of v1, /device:TPU:1, one launch (start us, length us, event | category | flops | bytes accessed | tf_op | source)
XLA Modules:
  0.0 288.2 jit_solution(18312590891655294601)
XLA Ops:
  14.1 2.4 gather_fusion
  16.8 33.3 %scatter_fusion = bf16[32,16,2048]{2,1,0:T(8,128)(2,1)S(1)} fusion(bf16[32,16,2048]{2,1,0:T(8,128)(2,1)S(1)} %broadcast_in_dim.21, s32[256]{0:T(256)S(1)} %bitcast.128, bf16[256,2048]{1,0:T(8,128)(2,1)} %gather_fusion), kind=kCustom, calls=%fused_computation.2 | custom fusion | bytes 3147776 | tf_op jit(solution)/shard_map/scatter | solution.py:136
  50.8 16.7 %all-to-all-start = ((bf16[32,1,16,128]{3,2,1,0:T(8,128)(2,1)}), bf16[32,1,16,128]{3,2,1,0:T(8,128)(2,1)S(1)}, u32[]{:S(2)}, u32[]{:S(2)}) async-start(bf16[32,1,16,128]{3,2,1,0:T(8,128)(2,1)} %dynamic-slice_bitcast_fusion), calls=%async_computation | async-start | bytes 262144 | tf_op jit(solution)/shard_map/all_to_all | solution.py:149
  68.9 21.1 %all-gather.2.cloned.1.call-done = bf16[4096,129]{0,1:T(8,128)(2,1)} async-done(((bf16[128,129]{0,1:T(8,128)(2,1)}), bf16[4096,129]{0,1:T(8,128)(2,1)}) %all-gather.2.cloned.1.call-update) | async-done | bytes 1056784 | tf_op jit(solution)/shard_map/all_gather | solution.py:30
  90.0 19.2 %conditional.1 = (f32[32,1,128,64]{2,3,0,1:T(8,128)}, f32[32,1,128]{2,1,0:T(1,128)S(1)}) conditional(s32[]{:T(128)} %convert_element_type.82, () %tuple.16, (s32[]{:T(128)}, s32[128]{0:T(128)S(1)}, bf16[4096,129]{0,1:T(8,128)(2,1)}, bf16[128,64]{0,1:T(8,128)(2,1)S(1)}) %tuple.17), branch_computations={%region_1.0_spmd, %region_2.5_spmd} | conditional | flops 219160704 | bytes 19064852 | solution.py:121
  94.4 2.4 copy.79
  96.7 9.9 %fusion.1 = bf16[128,32,128]{0,1,2:T(8,128)(2,1)S(1)} fusion(f32[128,32,128]{0,1,2:T(8,128)} %copy.79, s32[128]{0:T(128)S(1)} %broadcast_add_fusion, s32[32,128]{0,1:T(8,128)S(1)} %multiply_add_fusion), kind=kOutput, calls=%fused_computation.9 | output fusion | flops 78643200 | bytes 3162624 | tf_op jit(solution)/shard_map/cond/branch_1_fun/reduce_window_sum | solution.py:108
  106.7 2.6 convolution_bitcast_fusion
  110.7 3.2 %collective-permute-start = (bf16[128,64]{0,1:T(8,128)(2,1)S(1)}, bf16[128,64]{0,1:T(8,128)(2,1)S(1)}, u32[]{:S(2)}, u32[]{:S(2)}) collective-permute-start(bf16[128,64]{0,1:T(8,128)(2,1)S(1)} %multiply_reduce_fusion), channel_id=1, source_target_pairs={{0,1},{1,2},{2,3},{3,4},{4,5},{5,6},{6,7},{7,8},{8,9},{9,10},{10,1... | collective-permute-start | bytes 49160 | tf_op jit(solution)/shard_map/ppermute | solution.py:19
  113.9 4.6 %collective-permute-done = bf16[128,64]{0,1:T(8,128)(2,1)S(1)} collective-permute-done((bf16[128,64]{0,1:T(8,128)(2,1)S(1)}, bf16[128,64]{0,1:T(8,128)(2,1)S(1)}, u32[]{:S(2)}, u32[]{:S(2)}) %collective-permute-start) | collective-permute-done | bytes 16416 | tf_op jit(solution)/shard_map/ppermute | solution.py:19
  118.5 2.1 collective-permute-start.1
  120.6 6.7 %collective-permute-start.8 = (bf16[128,64]{0,1:T(8,128)(2,1)S(1)}, bf16[128,64]{0,1:T(8,128)(2,1)S(1)}, u32[]{:S(2)}, u32[]{:S(2)}) collective-permute-start(bf16[128,64]{0,1:T(8,128)(2,1)S(1)} %multiply_reduce_fusion), channel_id=1, source_target_pairs={{0,15},{1,0},{2,1},{3,2},{4,3},{5,4},{6,5},{7,6},{8,7},{9,8},{10,9... | collective-permute-start | bytes 49160 | tf_op jit(solution)/shard_map/ppermute | solution.py:21
  127.3 1.9 collective-permute-start.2
  129.3 6.7 %collective-permute-start.9 = (bf16[128,64]{0,1:T(8,128)(2,1)S(1)}, bf16[128,64]{0,1:T(8,128)(2,1)S(1)}, u32[]{:S(2)}, u32[]{:S(2)}) collective-permute-start(bf16[128,64]{0,1:T(8,128)(2,1)S(1)} %collective-permute-done.8), channel_id=1, source_target_pairs={{0,15},{1,0},{2,1},{3,2},{4,3},{5,4},{6,5},{7,6},{8,7},{9,8},{10,9... | collective-permute-start | bytes 49160 | tf_op jit(solution)/shard_map/ppermute | solution.py:21
  136.0 1.9 collective-permute-start.3
  139.7 6.3 %all-to-all-start.1 = ((bf16[16,32,1,16,128]{4,3,1,2,0:T(8,128)(2,1)}), bf16[16,32,1,16,128]{4,3,1,2,0:T(8,128)(2,1)S(1)}, u32[]{:S(2)}, u32[]{:S(2)}) async-start(bf16[16,32,1,16,128]{4,3,1,2,0:T(8,128)(2,1)} %broadcast_in_dim.22), calls=%async_computation.1 | async-start | bytes 4194304 | tf_op jit(solution)/shard_map/all_to_all | solution.py:42
  146.0 6.6 %collective-permute-start.10 = (bf16[128,64]{0,1:T(8,128)(2,1)S(1)}, bf16[128,64]{0,1:T(8,128)(2,1)S(1)}, u32[]{:S(2)}, u32[]{:S(2)}) collective-permute-start(bf16[128,64]{0,1:T(8,128)(2,1)S(1)} %collective-permute-done.9), channel_id=1, source_target_pairs={{0,15},{1,0},{2,1},{3,2},{4,3},{5,4},{6,5},{7,6},{8,7},{9,8},{10,9... | collective-permute-start | bytes 49160 | tf_op jit(solution)/shard_map/ppermute | solution.py:21
  152.6 1.9 collective-permute-start.4
  154.6 13.5 %collective-permute-done.10 = bf16[128,64]{0,1:T(8,128)(2,1)S(1)} collective-permute-done((bf16[128,64]{0,1:T(8,128)(2,1)S(1)}, bf16[128,64]{0,1:T(8,128)(2,1)S(1)}, u32[]{:S(2)}, u32[]{:S(2)}) %collective-permute-start.10) | collective-permute-done | bytes 16416 | tf_op jit(solution)/shard_map/ppermute | solution.py:21
  168.1 6.7 %collective-permute-start.11 = (bf16[128,64]{0,1:T(8,128)(2,1)S(1)}, bf16[128,64]{0,1:T(8,128)(2,1)S(1)}, u32[]{:S(2)}, u32[]{:S(2)}) collective-permute-start(bf16[128,64]{0,1:T(8,128)(2,1)S(1)} %collective-permute-done.10), channel_id=1, source_target_pairs={{0,15},{1,0},{2,1},{3,2},{4,3},{5,4},{6,5},{7,6},{8,7},{9,8},{10,9... | collective-permute-start | bytes 49160 | tf_op jit(solution)/shard_map/ppermute | solution.py:21
  174.9 1.9 collective-permute-start.5
  176.9 6.7 %collective-permute-start.12 = (bf16[128,64]{0,1:T(8,128)(2,1)S(1)}, bf16[128,64]{0,1:T(8,128)(2,1)S(1)}, u32[]{:S(2)}, u32[]{:S(2)}) collective-permute-start(bf16[128,64]{0,1:T(8,128)(2,1)S(1)} %collective-permute-done.11), channel_id=1, source_target_pairs={{0,15},{1,0},{2,1},{3,2},{4,3},{5,4},{6,5},{7,6},{8,7},{9,8},{10,9... | collective-permute-start | bytes 49160 | tf_op jit(solution)/shard_map/ppermute | solution.py:21
  185.6 6.7 %collective-permute-start.13 = (bf16[128,64]{0,1:T(8,128)(2,1)S(1)}, bf16[128,64]{0,1:T(8,128)(2,1)}, u32[]{:S(2)}, u32[]{:S(2)}) collective-permute-start(bf16[128,64]{0,1:T(8,128)(2,1)S(1)} %collective-permute-done.12), channel_id=1, source_target_pairs={{0,15},{1,0},{2,1},{3,2},{4,3},{5,4},{6,5},{7,6},{8,7},{9,8},{10,9... | collective-permute-start | bytes 49160 | tf_op jit(solution)/shard_map/ppermute | solution.py:21
  194.4 6.7 %collective-permute-start.14 = (bf16[128,64]{0,1:T(8,128)(2,1)}, bf16[128,64]{0,1:T(8,128)(2,1)}, u32[]{:S(2)}, u32[]{:S(2)}) collective-permute-start(bf16[128,64]{0,1:T(8,128)(2,1)} %collective-permute-done.13), channel_id=1, source_target_pairs={{0,15},{1,0},{2,1},{3,2},{4,3},{5,4},{6,5},{7,6},{8,7},{9,8},{10,9... | collective-permute-start | bytes 49160 | tf_op jit(solution)/shard_map/ppermute | solution.py:21
  201.2 3.8 %copy.90 = bf16[32,1,16,16,128]{4,3,2,0,1:T(8,128)(2,1)} copy(bf16[32,1,16,16,128]{4,2,0,1,3:T(8,128)(2,1)S(1)} %bitcast.130) | data formatting | bytes 4194304 | tf_op jit(solution)/shard_map/transpose | solution.py:37
  205.1 2.8 reshape.363
  211.5 3.9 %all-to-all-start.2 = ((bf16[16,32,1,16,128]{4,3,1,2,0:T(8,128)(2,1)}), bf16[16,32,1,16,128]{4,3,1,2,0:T(8,128)(2,1)S(1)}, u32[]{:S(2)}, u32[]{:S(2)}) async-start(bf16[16,32,1,16,128]{4,3,1,2,0:T(8,128)(2,1)} %broadcast_in_dim.23), calls=%async_computation.2 | async-start | bytes 4194304 | tf_op jit(solution)/shard_map/all_to_all | solution.py:42
  217.1 22.3 %all-to-all-done.2 = bf16[16,32,1,16,128]{4,3,1,2,0:T(8,128)(2,1)S(1)} async-done(((bf16[16,32,1,16,128]{4,3,1,2,0:T(8,128)(2,1)}), bf16[16,32,1,16,128]{4,3,1,2,0:T(8,128)(2,1)S(1)}, u32[]{:S(2)}, u32[]{:S(2)}) %all-to-all-start.2) | async-done | bytes 2097184 | tf_op jit(solution)/shard_map/all_to_all | solution.py:42
  239.4 3.8 %copy.91 = bf16[32,1,16,16,128]{4,3,2,0,1:T(8,128)(2,1)} copy(bf16[32,1,16,16,128]{4,2,0,1,3:T(8,128)(2,1)S(1)} %bitcast.131) | data formatting | bytes 4194304 | tf_op jit(solution)/shard_map/transpose | solution.py:37
  243.1 2.9 reshape.366
  247.4 15.6 %all-to-all-start.3 = ((bf16[32,1,16,128]{3,2,1,0:T(8,128)(2,1)}), bf16[32,1,16,128]{3,2,1,0:T(8,128)(2,1)S(1)}, u32[]{:S(2)}, u32[]{:S(2)}) async-start(bf16[32,1,16,128]{3,2,1,0:T(8,128)(2,1)} %fusion.22), calls=%async_computation.3 | async-start | bytes 262144 | tf_op jit(solution)/shard_map/all_to_all | solution.py:157
  268.1 10.8 %all-to-all-done.3 = bf16[32,1,16,128]{3,2,1,0:T(8,128)(2,1)S(1)} async-done(((bf16[32,1,16,128]{3,2,1,0:T(8,128)(2,1)}), bf16[32,1,16,128]{3,2,1,0:T(8,128)(2,1)S(1)}, u32[]{:S(2)}, u32[]{:S(2)}) %all-to-all-start.3) | async-done | bytes 131104 | tf_op jit(solution)/shard_map/all_to_all | solution.py:157
  (169 shorter events, 34.9 us)
Async XLA Ops:
  7.2 200.7 %copy-start = (bf16[1,2048,128]{2,1,0:T(8,128)(2,1)S(1)}, bf16[1,2048,128]{2,1,0:T(8,128)(2,1)}, u32[]{:S(2)}) copy-start(bf16[1,2048,128]{2,1,0:T(8,128)(2,1)} %param.29) | copy-start | bytes 1572868
  7.2 82.8 %all-gather.2.cloned.1.call-start = ((), (), s32[]{:S(2)}) async-start(), calls=%async_computation.4 | async-start | bytes 1148928 | tf_op jit(solution)/shard_map/all_gather | solution.py:30
  16.8 50.8 %copy-start.2 = (bf16[128,2048]{1,0:T(8,128)(2,1)S(1)}, bf16[128,2048]{1,0:T(8,128)(2,1)}, u32[]{:S(2)}) copy-start(bf16[128,2048]{1,0:T(8,128)(2,1)} %param.17) | copy-start | bytes 1572868
  16.8 50.8 %copy-start.33 = (f32[2048]{0:T(1024)S(1)}, f32[2048]{0:T(1024)}, u32[]{:S(2)}) copy-start(f32[2048]{0:T(1024)} %param.18) | copy-start | bytes 24580
  50.8 87.2 %all-to-all-start = ((bf16[32,1,16,128]{3,2,1,0:T(8,128)(2,1)}), bf16[32,1,16,128]{3,2,1,0:T(8,128)(2,1)S(1)}, u32[]{:S(2)}, u32[]{:S(2)}) async-start(bf16[32,1,16,128]{3,2,1,0:T(8,128)(2,1)} %dynamic-slice_bitcast_fusion), calls=%async_computation | async-start | bytes 262144 | tf_op jit(solution)/shard_map/all_to_all | solution.py:149
  90.0 39.2 %copy-start.28 = (f32[128,4]{0,1:T(4,128)S(1)}, f32[128,4]{0,1:T(4,128)}, u32[]{:S(2)}) copy-start(f32[128,4]{0,1:T(4,128)} %param.27) | copy-start | bytes 6148
  110.7 7.8 %collective-permute-start = (bf16[128,64]{0,1:T(8,128)(2,1)S(1)}, bf16[128,64]{0,1:T(8,128)(2,1)S(1)}, u32[]{:S(2)}, u32[]{:S(2)}) collective-permute-start(bf16[128,64]{0,1:T(8,128)(2,1)S(1)} %multiply_reduce_fusion), channel_id=1, source_target_pairs={{0,1},{1,2},{2,3},{3,4},{4,5},{5,6},{6,7},{7,8},{8,9},{9,10},{10,1... | collective-permute-start | bytes 49160 | tf_op jit(solution)/shard_map/ppermute | solution.py:19
  118.5 8.8 %collective-permute-start.1 = (bf16[128,64]{0,1:T(8,128)(2,1)S(1)}, bf16[128,64]{0,1:T(8,128)(2,1)S(1)}, u32[]{:S(2)}, u32[]{:S(2)}) collective-permute-start(bf16[128,64]{0,1:T(8,128)(2,1)S(1)} %collective-permute-done), channel_id=1, source_target_pairs={{0,1},{1,2},{2,3},{3,4},{4,5},{5,6},{6,7},{7,8},{8,9},{9,10},{10,1... | collective-permute-start | bytes 49160 | tf_op jit(solution)/shard_map/ppermute | solution.py:19
  120.6 8.7 %collective-permute-start.8 = (bf16[128,64]{0,1:T(8,128)(2,1)S(1)}, bf16[128,64]{0,1:T(8,128)(2,1)S(1)}, u32[]{:S(2)}, u32[]{:S(2)}) collective-permute-start(bf16[128,64]{0,1:T(8,128)(2,1)S(1)} %multiply_reduce_fusion), channel_id=1, source_target_pairs={{0,15},{1,0},{2,1},{3,2},{4,3},{5,4},{6,5},{7,6},{8,7},{9,8},{10,9... | collective-permute-start | bytes 49160 | tf_op jit(solution)/shard_map/ppermute | solution.py:21
  127.3 8.7 %collective-permute-start.2 = (bf16[128,64]{0,1:T(8,128)(2,1)S(1)}, bf16[128,64]{0,1:T(8,128)(2,1)S(1)}, u32[]{:S(2)}, u32[]{:S(2)}) collective-permute-start(bf16[128,64]{0,1:T(8,128)(2,1)S(1)} %collective-permute-done.1), channel_id=1, source_target_pairs={{0,1},{1,2},{2,3},{3,4},{4,5},{5,6},{6,7},{7,8},{8,9},{9,10},{10,1... | collective-permute-start | bytes 49160 | tf_op jit(solution)/shard_map/ppermute | solution.py:19
  129.3 16.7 %collective-permute-start.9 = (bf16[128,64]{0,1:T(8,128)(2,1)S(1)}, bf16[128,64]{0,1:T(8,128)(2,1)S(1)}, u32[]{:S(2)}, u32[]{:S(2)}) collective-permute-start(bf16[128,64]{0,1:T(8,128)(2,1)S(1)} %collective-permute-done.8), channel_id=1, source_target_pairs={{0,15},{1,0},{2,1},{3,2},{4,3},{5,4},{6,5},{7,6},{8,7},{9,8},{10,9... | collective-permute-start | bytes 49160 | tf_op jit(solution)/shard_map/ppermute | solution.py:21
  136.0 65.1 %copy-start.8 = (bf16[128,64]{0,1:T(8,128)(2,1)}, bf16[128,64]{0,1:T(8,128)(2,1)S(1)}, u32[]{:S(2)}) copy-start(bf16[128,64]{0,1:T(8,128)(2,1)S(1)} %collective-permute-done.2) | copy-start | bytes 49156
  136.0 16.6 %collective-permute-start.3 = (bf16[128,64]{0,1:T(8,128)(2,1)S(1)}, bf16[128,64]{0,1:T(8,128)(2,1)S(1)}, u32[]{:S(2)}, u32[]{:S(2)}) collective-permute-start(bf16[128,64]{0,1:T(8,128)(2,1)S(1)} %collective-permute-done.2), channel_id=1, source_target_pairs={{0,1},{1,2},{2,3},{3,4},{4,5},{5,6},{6,7},{7,8},{8,9},{9,10},{10,1... | collective-permute-start | bytes 49160 | tf_op jit(solution)/shard_map/ppermute | solution.py:19
  139.7 37.1 %copy-start.30 = (f32[128,2]{0,1:T(2,128)S(1)}, f32[128,2]{0,1:T(2,128)}, u32[]{:S(2)}) copy-start(f32[128,2]{0,1:T(2,128)} %param.28) | copy-start | bytes 3076
  139.7 61.5 %all-to-all-start.1 = ((bf16[16,32,1,16,128]{4,3,1,2,0:T(8,128)(2,1)}), bf16[16,32,1,16,128]{4,3,1,2,0:T(8,128)(2,1)S(1)}, u32[]{:S(2)}, u32[]{:S(2)}) async-start(bf16[16,32,1,16,128]{4,3,1,2,0:T(8,128)(2,1)} %broadcast_in_dim.22), calls=%async_computation.1 | async-start | bytes 4194304 | tf_op jit(solution)/shard_map/all_to_all | solution.py:42
  146.0 59.0 %copy-start.6 = (bf16[128,64]{0,1:T(8,128)(2,1)}, bf16[128,64]{0,1:T(8,128)(2,1)S(1)}, u32[]{:S(2)}) copy-start(bf16[128,64]{0,1:T(8,128)(2,1)S(1)} %collective-permute-done.9) | copy-start | bytes 49156
  146.0 22.1 %collective-permute-start.10 = (bf16[128,64]{0,1:T(8,128)(2,1)S(1)}, bf16[128,64]{0,1:T(8,128)(2,1)S(1)}, u32[]{:S(2)}, u32[]{:S(2)}) collective-permute-start(bf16[128,64]{0,1:T(8,128)(2,1)S(1)} %collective-permute-done.9), channel_id=1, source_target_pairs={{0,15},{1,0},{2,1},{3,2},{4,3},{5,4},{6,5},{7,6},{8,7},{9,8},{10,9... | collective-permute-start | bytes 49160 | tf_op jit(solution)/shard_map/ppermute | solution.py:21
  152.6 52.4 %copy-start.10 = (bf16[128,64]{0,1:T(8,128)(2,1)}, bf16[128,64]{0,1:T(8,128)(2,1)S(1)}, u32[]{:S(2)}) copy-start(bf16[128,64]{0,1:T(8,128)(2,1)S(1)} %collective-permute-done.3) | copy-start | bytes 49156
  152.6 22.2 %collective-permute-start.4 = (bf16[128,64]{0,1:T(8,128)(2,1)S(1)}, bf16[128,64]{0,1:T(8,128)(2,1)S(1)}, u32[]{:S(2)}, u32[]{:S(2)}) collective-permute-start(bf16[128,64]{0,1:T(8,128)(2,1)S(1)} %collective-permute-done.3), channel_id=1, source_target_pairs={{0,1},{1,2},{2,3},{3,4},{4,5},{5,6},{6,7},{7,8},{8,9},{9,10},{10,1... | collective-permute-start | bytes 49160 | tf_op jit(solution)/shard_map/ppermute | solution.py:19
  168.1 36.9 %copy-start.12 = (bf16[128,64]{0,1:T(8,128)(2,1)}, bf16[128,64]{0,1:T(8,128)(2,1)S(1)}, u32[]{:S(2)}) copy-start(bf16[128,64]{0,1:T(8,128)(2,1)S(1)} %collective-permute-done.10) | copy-start | bytes 49156
  168.1 8.7 %collective-permute-start.11 = (bf16[128,64]{0,1:T(8,128)(2,1)S(1)}, bf16[128,64]{0,1:T(8,128)(2,1)S(1)}, u32[]{:S(2)}, u32[]{:S(2)}) collective-permute-start(bf16[128,64]{0,1:T(8,128)(2,1)S(1)} %collective-permute-done.10), channel_id=1, source_target_pairs={{0,15},{1,0},{2,1},{3,2},{4,3},{5,4},{6,5},{7,6},{8,7},{9,8},{10,9... | collective-permute-start | bytes 49160 | tf_op jit(solution)/shard_map/ppermute | solution.py:21
  174.9 30.1 %copy-start.19 = (bf16[128,64]{0,1:T(8,128)(2,1)}, bf16[128,64]{0,1:T(8,128)(2,1)S(1)}, u32[]{:S(2)}) copy-start(bf16[128,64]{0,1:T(8,128)(2,1)S(1)} %collective-permute-done.4) | copy-start | bytes 49156
  174.9 8.7 %collective-permute-start.5 = (bf16[128,64]{0,1:T(8,128)(2,1)S(1)}, bf16[128,64]{0,1:T(8,128)(2,1)S(1)}, u32[]{:S(2)}, u32[]{:S(2)}) collective-permute-start(bf16[128,64]{0,1:T(8,128)(2,1)S(1)} %collective-permute-done.4), channel_id=1, source_target_pairs={{0,1},{1,2},{2,3},{3,4},{4,5},{5,6},{6,7},{7,8},{8,9},{9,10},{10,1... | collective-permute-start | bytes 49160 | tf_op jit(solution)/shard_map/ppermute | solution.py:19
  176.9 28.1 %copy-start.17 = (bf16[128,64]{0,1:T(8,128)(2,1)}, bf16[128,64]{0,1:T(8,128)(2,1)S(1)}, u32[]{:S(2)}) copy-start(bf16[128,64]{0,1:T(8,128)(2,1)S(1)} %collective-permute-done.11) | copy-start | bytes 49156
  176.9 8.7 %collective-permute-start.12 = (bf16[128,64]{0,1:T(8,128)(2,1)S(1)}, bf16[128,64]{0,1:T(8,128)(2,1)S(1)}, u32[]{:S(2)}, u32[]{:S(2)}) collective-permute-start(bf16[128,64]{0,1:T(8,128)(2,1)S(1)} %collective-permute-done.11), channel_id=1, source_target_pairs={{0,15},{1,0},{2,1},{3,2},{4,3},{5,4},{6,5},{7,6},{8,7},{9,8},{10,9... | collective-permute-start | bytes 49160 | tf_op jit(solution)/shard_map/ppermute | solution.py:21
  183.6 8.7 %collective-permute-start.6 = (bf16[128,64]{0,1:T(8,128)(2,1)S(1)}, bf16[128,64]{0,1:T(8,128)(2,1)S(1)}, u32[]{:S(2)}, u32[]{:S(2)}) collective-permute-start(bf16[128,64]{0,1:T(8,128)(2,1)S(1)} %collective-permute-done.5), channel_id=1, source_target_pairs={{0,1},{1,2},{2,3},{3,4},{4,5},{5,6},{6,7},{7,8},{8,9},{9,10},{10,1... | collective-permute-start | bytes 49160 | tf_op jit(solution)/shard_map/ppermute | solution.py:19
  185.6 8.8 %collective-permute-start.13 = (bf16[128,64]{0,1:T(8,128)(2,1)S(1)}, bf16[128,64]{0,1:T(8,128)(2,1)}, u32[]{:S(2)}, u32[]{:S(2)}) collective-permute-start(bf16[128,64]{0,1:T(8,128)(2,1)S(1)} %collective-permute-done.12), channel_id=1, source_target_pairs={{0,15},{1,0},{2,1},{3,2},{4,3},{5,4},{6,5},{7,6},{8,7},{9,8},{10,9... | collective-permute-start | bytes 49160 | tf_op jit(solution)/shard_map/ppermute | solution.py:21
  192.3 8.8 %collective-permute-start.7 = (bf16[128,64]{0,1:T(8,128)(2,1)S(1)}, bf16[128,64]{0,1:T(8,128)(2,1)S(1)}, u32[]{:S(2)}, u32[]{:S(2)}) collective-permute-start(bf16[128,64]{0,1:T(8,128)(2,1)S(1)} %collective-permute-done.6), channel_id=1, source_target_pairs={{0,1},{1,2},{2,3},{3,4},{4,5},{5,6},{6,7},{7,8},{8,9},{9,10},{10,1... | collective-permute-start | bytes 49160 | tf_op jit(solution)/shard_map/ppermute | solution.py:19
  194.4 21.8 %collective-permute-start.14 = (bf16[128,64]{0,1:T(8,128)(2,1)}, bf16[128,64]{0,1:T(8,128)(2,1)}, u32[]{:S(2)}, u32[]{:S(2)}) collective-permute-start(bf16[128,64]{0,1:T(8,128)(2,1)} %collective-permute-done.13), channel_id=1, source_target_pairs={{0,15},{1,0},{2,1},{3,2},{4,3},{5,4},{6,5},{7,6},{8,7},{9,8},{10,9... | collective-permute-start | bytes 49160 | tf_op jit(solution)/shard_map/ppermute | solution.py:21
  211.5 27.9 %all-to-all-start.2 = ((bf16[16,32,1,16,128]{4,3,1,2,0:T(8,128)(2,1)}), bf16[16,32,1,16,128]{4,3,1,2,0:T(8,128)(2,1)S(1)}, u32[]{:S(2)}, u32[]{:S(2)}) async-start(bf16[16,32,1,16,128]{4,3,1,2,0:T(8,128)(2,1)} %broadcast_in_dim.23), calls=%async_computation.2 | async-start | bytes 4194304 | tf_op jit(solution)/shard_map/all_to_all | solution.py:42
  217.1 22.3 %copy-start.5 = (bf16[128,2048]{0,1:T(8,128)(2,1)}, bf16[128,2048]{0,1:T(8,128)(2,1)S(1)}, u32[]{:S(2)}) copy-start(bf16[128,2048]{0,1:T(8,128)(2,1)S(1)} %constant_dynamic-update-slice_fusion.3) | copy-start | bytes 1572868
  247.4 31.4 %all-to-all-start.3 = ((bf16[32,1,16,128]{3,2,1,0:T(8,128)(2,1)}), bf16[32,1,16,128]{3,2,1,0:T(8,128)(2,1)S(1)}, u32[]{:S(2)}, u32[]{:S(2)}) async-start(bf16[32,1,16,128]{3,2,1,0:T(8,128)(2,1)} %fusion.22), calls=%async_computation.3 | async-start | bytes 262144 | tf_op jit(solution)/shard_map/all_to_all | solution.py:157
  (22 other events, 171.7 us)
Sparse Core Ops, SparseCore 0:
  12.4 77.6 all-gather.1
